TPU v7x, 512 devices: a whole 4x4x16 slice. The times are simulated.
512 devices in a mesh: sp: 32 (over z, core), tp: 16 (over y, x).
Axes of the slice: x: 4, y: 4, z: 16, core: 2. Of those that a mesh axis runs over, the one named last changes fastest.
Arguments:
- moe_input: bfloat16 [6144, 2048], P('sp'), may hold values from -6 to 6
- out_grad: bfloat16 [6144, 2048], P('sp'), may hold values from -6 to 6
- route_ids: int32 [6144, 2], P('sp'), may hold values from 0 to 31, all different within a row; in each aligned block of 192 rows (0 to 191, 192 to 383, ...) at most 18 rows name the same one
- route_weights: float32 [6144, 2], P('sp'), may hold values from 0.2 to 2
- expert_gate: bfloat16 [32, 2048, 2048], P('sp', None, 'tp'), may hold values from -0.125 to 0.125
- expert_up: bfloat16 [32, 2048, 2048], P('sp', None, 'tp'), may hold values from -0.125 to 0.125
- expert_down: bfloat16 [32, 2048, 2048], P('sp', 'tp'), may hold values from -0.125 to 0.125
- proj_weight: bfloat16 [1024, 2048], P(None, 'tp'), may hold values from -0.1875 to 0.1875
- glu_value: bfloat16 [1024, 6144], P('tp', 'sp'), may hold values from -6 to 6
- glu_gate: bfloat16 [1024, 6144], P('tp', 'sp'), may hold values from -8 to 8
- conv_taps: float32 [1024, 31], P('tp'), may hold values from -1 to 1
- norm_input: bfloat16 [1024, 6144], P('tp', 'sp'), may hold values from -6 to 6
- norm_gain: float32 [1024], replicated, may hold values from 0.1 to 1.9
Outputs:
- grad_gate: bfloat16 [32, 2048, 2048], P('sp', None, 'tp')
- grad_up: bfloat16 [32, 2048, 2048], P('sp', None, 'tp')
- grad_down: bfloat16 [32, 2048, 2048], P('sp', 'tp')
- grad_proj: float32 [1024, 2048], P('sp', 'tp')
- grad_value: bfloat16 [1024, 6144], P('tp', 'sp')
- grad_glu_gate: bfloat16 [1024, 6144], P('tp', 'sp')
Inputs may be any that keep to these rules, and one draw needn't show every extreme that they name: `route_ids`: within the rows of one device, the 2 ids of a position differ and no expert is named by more than 18 pairs; some expert is named by exactly 18.
All inputs are finite; a program needn't handle non-finite values.
Results may differ from a plain program's by a relative error of at most 0.025.
Values may be sent and summed in bfloat16 or wider, within the bound.
No kernel may reach another device: no remote copies, remote signals or barrier semaphores. Data moves between devices by JAX's collectives and lax.ppermute only.
A program may use at most 64 MiB of HBM per device.

v0:
```python
import jax
import jax.numpy as jnp
from jax import lax
from jax.sharding import Mesh
from jax.sharding import PartitionSpec as P

TP = ("tp_0", "tp_1")
norm_eps = 1e-05


def sent_together(arrays, axis, split_dim, concat_dim, along):
    ends, at = ([], 0)
    for a in arrays[:-1]:
        at += a.shape[along]
        ends.append(at)
    both = jnp.concatenate(arrays, axis=along)
    return tuple(
        jnp.split(
            lax.all_to_all(both, axis, split_axis=split_dim, concat_axis=concat_dim, tiled=True),
            ends,
            axis=along,
        )
    )


def sent_together_2(arrays, axis, dim, along):
    ends, at = ([], 0)
    for a in arrays[:-1]:
        at += a.shape[along]
        ends.append(at)
    both = jnp.concatenate(arrays, axis=along)
    return tuple(jnp.split(lax.all_gather(both, axis, axis=dim, tiled=True), ends, axis=along))


def in_blocks(shard, dim, length):
    before, after = (shard.shape[:dim], shard.shape[dim + 1 :])
    return jnp.moveaxis(shard.reshape(*before, length, -1, *after), dim, 0)


def sum_at_owner(shard, axis, dim):
    length = lax.axis_size(axis)
    blocks = lax.all_to_all(in_blocks(shard, dim, length), axis, 0, 0, tiled=True)
    return jnp.sum(blocks.astype(jnp.float32), axis=0)


def from_everyone(shard, axis):
    length = lax.axis_size(axis)
    return lax.all_to_all(
        jnp.broadcast_to(shard[None], (length, *shard.shape)), axis, 0, 0, tiled=True
    )


def laid_out(blocks, dim):
    blocks = jnp.moveaxis(blocks, 0, dim)
    shape = blocks.shape
    return blocks.reshape(*shape[:dim], shape[dim] * shape[dim + 1], *shape[dim + 2 :])


def gather_directly(shard, axis, dim):
    blocks = from_everyone(shard, axis)
    return laid_out(blocks, dim)


def over_axes(shard, axes):
    for axis in axes:
        shard = lax.psum(shard, axis)
    return shard


def shifted(shard, axis, by):
    length = lax.axis_size(axis)
    pairs = [(i, i + by) for i in range(length) if 0 <= i + by < length]
    return lax.ppermute(shard, axis, pairs)


def silu_grad(pre):
    sigmoid_pre = jax.nn.sigmoid(pre)
    return sigmoid_pre * (1.0 + pre * (1.0 - sigmoid_pre))


def slot_table(route_ids, route_weights, experts, capacity):
    tok_rows, top_count = route_ids.shape
    flat_ids = route_ids.reshape(-1)
    onehot = (flat_ids[:, None] == jnp.arange(experts, dtype=jnp.int32)[None, :]).astype(jnp.int32)
    before = jnp.cumsum(onehot, axis=0) - onehot
    slot_index = jnp.sum(before * onehot, axis=1)
    target = flat_ids * capacity + slot_index
    buffer_rows = jnp.arange(experts * capacity, dtype=jnp.int32)
    matches = (buffer_rows[:, None] == target[None, :]).reshape(
        experts * capacity, tok_rows, top_count
    )
    placing = jnp.sum(matches.astype(jnp.float32), axis=2).astype(jnp.bfloat16)
    slot_scale = jnp.sum(jnp.where(matches, route_weights[None, :, :], 0.0), axis=(1, 2))
    return (placing, slot_scale)


def body(
    moe_input,
    out_grad,
    route_ids,
    route_weights,
    expert_gate,
    expert_up,
    expert_down,
    proj_weight,
    glu_value,
    glu_gate,
    conv_taps,
    norm_input,
    norm_gain,
):
    groups = lax.axis_size("sp")
    lane_count = lax.axis_size(TP)
    lane_index = lax.axis_index(TP)
    tok_rows, model_width = moe_input.shape
    top_count = route_ids.shape[1]
    capacity = tok_rows * top_count * 3 // (2 * groups)
    part_width = model_width // lane_count
    placing, slot_scale = slot_table(route_ids, route_weights, groups, capacity)
    own_grad = lax.dynamic_slice_in_dim(out_grad, lane_index * part_width, part_width, 1)
    own_input = lax.dynamic_slice_in_dim(moe_input, lane_index * part_width, part_width, 1)
    sent_rows = jnp.dot(placing, own_input, preferred_element_type=jnp.float32).astype(jnp.bfloat16)
    sent_grad = (
        jnp.dot(placing, own_grad, preferred_element_type=jnp.float32) * slot_scale[:, None]
    ).astype(jnp.bfloat16)
    part_rows, part_grad = sent_together(
        (
            sent_rows.reshape(groups, capacity, part_width),
            sent_grad.reshape(groups, capacity, part_width),
        ),
        "sp",
        0,
        0,
        1,
    )
    arrived_rows, arrived_grad = sent_together_2((part_rows, part_grad), TP, 2, 0)
    token_rows = arrived_rows.reshape(-1, model_width)
    grad_rows = arrived_grad.reshape(-1, model_width)
    w_gate = expert_gate[0]
    w_up = expert_up[0]
    w_down = expert_down[0]
    gate_pre = jnp.dot(token_rows, w_gate, preferred_element_type=jnp.float32)
    up_pre = jnp.dot(token_rows, w_up, preferred_element_type=jnp.float32)
    gate_act = jax.nn.silu(gate_pre)
    hidden = (gate_act * up_pre).astype(jnp.bfloat16)
    down_grad = lax.dot_general(
        hidden, grad_rows, (((0,), (0,)), ((), ())), preferred_element_type=jnp.float32
    ).astype(jnp.bfloat16)
    grad_hidden = lax.dot_general(
        grad_rows, w_down, (((1,), (1,)), ((), ())), preferred_element_type=jnp.float32
    )
    gate_grad = (grad_hidden * up_pre * silu_grad(gate_pre)).astype(jnp.bfloat16)
    up_grad = (grad_hidden * gate_act).astype(jnp.bfloat16)
    gate_wgrad = lax.dot_general(
        token_rows, gate_grad, (((0,), (0,)), ((), ())), preferred_element_type=jnp.float32
    ).astype(jnp.bfloat16)
    up_wgrad = lax.dot_general(
        token_rows, up_grad, (((0,), (0,)), ((), ())), preferred_element_type=jnp.float32
    ).astype(jnp.bfloat16)
    input_grad = lax.dot_general(
        gate_grad, w_gate, (((1,), (1,)), ((), ())), preferred_element_type=jnp.float32
    )
    input_grad = input_grad + lax.dot_general(
        up_grad, w_up, (((1,), (1,)), ((), ())), preferred_element_type=jnp.float32
    )
    summed_grad = sum_at_owner(input_grad.astype(jnp.bfloat16), TP, 1).astype(jnp.bfloat16)
    returned = lax.all_to_all(
        summed_grad.reshape(groups, capacity, part_width),
        "sp",
        split_axis=0,
        concat_axis=0,
        tiled=True,
    )
    moe_grad = lax.dot_general(
        placing,
        returned.reshape(-1, part_width),
        (((0,), (0,)), ((), ())),
        preferred_element_type=jnp.float32,
    )
    mix_grad = (own_grad.astype(jnp.float32) + moe_grad).astype(jnp.bfloat16)
    channel_part = norm_input.shape[0]
    conv_values = gather_directly(norm_input, TP, 0).astype(jnp.float32)
    channels = conv_values.shape[0]
    centred = conv_values - jnp.mean(conv_values, axis=0, keepdims=True)
    inv_scale = lax.rsqrt(jnp.mean(centred * centred, axis=0, keepdims=True) + norm_eps)
    normed = centred * inv_scale
    scaled = normed * norm_gain[:, None]
    act = jax.nn.silu(scaled).astype(jnp.bfloat16)
    grad_proj = sum_at_owner(
        jnp.dot(act, mix_grad, preferred_element_type=jnp.float32).astype(jnp.bfloat16), "sp", 0
    )
    act_partial = lax.dot_general(
        proj_weight, mix_grad, (((1,), (1,)), ((), ())), preferred_element_type=jnp.float32
    )
    grad_act = sum_at_owner(act_partial.astype(jnp.bfloat16), TP, 0)
    normed_own = lax.dynamic_slice_in_dim(normed, lane_index * channel_part, channel_part, 0)
    scaled_own = lax.dynamic_slice_in_dim(scaled, lane_index * channel_part, channel_part, 0)
    gain_own = lax.dynamic_slice_in_dim(norm_gain, lane_index * channel_part, channel_part, 0)
    grad_normed = grad_act * silu_grad(scaled_own) * gain_own[:, None]
    sum_grad, sum_cross = (
        over_axes(jnp.sum(grad_normed, axis=0), TP),
        over_axes(jnp.sum(grad_normed * normed_own, axis=0), TP),
    )
    grad_conv = inv_scale * (
        grad_normed - sum_grad[None, :] / channels - normed_own * (sum_cross[None, :] / channels)
    )
    taps_count = conv_taps.shape[1]
    reach_back = taps_count - 1
    ahead_rows = shifted(grad_conv[:, :reach_back], "sp", -1)
    extended = jnp.concatenate([grad_conv, ahead_rows], axis=1)
    grad_glu = jnp.zeros_like(grad_conv)
    for tap_index in range(taps_count):
        grad_glu = (
            grad_glu
            + conv_taps[:, tap_index : tap_index + 1]
            * extended[:, reach_back - tap_index : reach_back - tap_index + tok_rows]
        )
    sigmoid_gate = jax.nn.sigmoid(glu_gate.astype(jnp.float32))
    grad_value = (grad_glu * sigmoid_gate).astype(jnp.bfloat16)
    grad_glu_gate = (
        grad_glu * glu_value.astype(jnp.float32) * sigmoid_gate * (1.0 - sigmoid_gate)
    ).astype(jnp.bfloat16)
    return (gate_wgrad[None], up_wgrad[None], down_grad[None], grad_proj, grad_value, grad_glu_gate)


def solution(mesh):
    finer = Mesh(mesh.devices.reshape(mesh.shape["sp"], 4, 4), ("sp", "tp_0", "tp_1"))
    return jax.shard_map(
        body,
        mesh=finer,
        in_specs=(
            P("sp", None),
            P("sp", None),
            P("sp", None),
            P("sp", None),
            P("sp", None, TP),
            P("sp", None, TP),
            P("sp", TP, None),
            P(None, TP),
            P(TP, "sp"),
            P(TP, "sp"),
            P(TP, None),
            P(TP, "sp"),
            P(),
        ),
        out_specs=(
            P("sp", None, TP),
            P("sp", None, TP),
            P("sp", TP, None),
            P("sp", TP),
            P(TP, "sp"),
            P(TP, "sp"),
        ),
        check_vma=False,
    )
```

profile of v0, /device:TPU:1, one launch (start us, length us, event | category | flops | bytes accessed | tf_op | source)
XLA Modules:
  0.0 290.6 jit_solution(6470165151364125645)
XLA Ops:
  7.2 0.9 copy.44
  8.4 0.9 reduce-window.6
  9.9 0.7 multiply_add_fusion
  10.6 0.9 convert_reduce_fusion.1
  11.5 1.1 fusion.5
  13.1 41.5 %all_to_all.30 = bf16[32,36,128]{2,1,0:T(8,128)(2,1)S(1)} all-to-all(bf16[32,36,128]{2,1,0:T(8,128)(2,1)S(1)} %pad_maximum_fusion.1), channel_id=1, replica_groups=mesh['sp'=32,'tp_0'=4,'tp_1'=4] {'sp'}, dimensions={0} | all-to-all | bytes 589824 | tf_op jit(solution)/shard_map/all_to_all | solution.py:19
  54.7 0.8 pad_maximum_fusion
  55.6 0.8 broadcast_in_dim.25
  56.4 6.8 %all-to-all-start.1 = ((bf16[16,64,192]{2,1,0:T(8,128)(2,1)}), bf16[16,64,192]{2,1,0:T(8,128)(2,1)}, u32[]{:S(2)}, u32[]{:S(2)}) async-start(bf16[16,64,192]{2,1,0:T(8,128)(2,1)} %broadcast_in_dim.25), calls=%async_computation.1 | async-start | bytes 1048576 | tf_op jit(solution)/shard_map/all_to_all | solution.py:48
  63.2 64.7 %all-gather.2.cloned.1.call-done = bf16[64,18,2048]{2,1,0:T(8,128)(2,1)} async-done(((bf16[64,18,128]{2,1,0:T(8,128)(2,1)}), bf16[64,18,2048]{2,1,0:T(8,128)(2,1)}) %all-gather.2.cloned.1.call-update) | async-done | bytes 4718608 | tf_op jit(solution)/shard_map/all_gather | solution.py:32
  128.0 6.6 %fusion.123 = (bf16[32,18,2048]{2,1,0:T(8,128)(2,1)}, bf16[32,18,2048]{2,1,0:T(8,128)(2,1)}) fusion(bf16[64,18,2048]{2,1,0:T(8,128)(2,1)} %all-gather.2.cloned.1.call-done), kind=kLoop, calls=%fused_computation.232 | loop fusion | bytes 9437184 | tf_op jit(solution)/shard_map/split | solution.py:32
  134.6 2.9 %reshape.106 = bf16[576,2048]{1,0:T(8,128)(2,1)S(1)} reshape(bf16[32,18,2048]{2,1,0:T(8,128)(2,1)} %get-tuple-element.18) | data formatting | bytes 4718592 | tf_op jit(solution)/shard_map/reshape | solution.py:137
  137.5 2.6 fusion.10
  140.1 1.5 fusion.13
  141.6 4.3 %reshape.107 = bf16[576,2048]{1,0:T(8,128)(2,1)} reshape(bf16[32,18,2048]{2,1,0:T(8,128)(2,1)} %get-tuple-element.17) | data formatting | bytes 4718592 | tf_op jit(solution)/shard_map/reshape | solution.py:138
  145.9 2.8 multiply_convert_fusion.3
  148.7 0.8 fusion.8
  149.9 0.8 fusion.3
  150.6 2.1 copy.54
  152.7 4.8 %all-to-all-start.2 = ((bf16[16,576,128]{2,1,0:T(8,128)(2,1)}), bf16[16,576,128]{2,1,0:T(8,128)(2,1)}, u32[]{:S(2)}, u32[]{:S(2)}) async-start(bf16[16,576,128]{2,1,0:T(8,128)(2,1)} %bitcast.138), calls=%async_computation.2 | async-start | bytes 4718592 | tf_op jit(solution)/shard_map/all_to_all | solution.py:42
  159.5 1.2 convert_reduce_fusion.2
  160.7 1.2 multiply_reduce_fusion
  161.9 26.0 %all-to-all-done.2 = bf16[16,576,128]{2,1,0:T(8,128)(2,1)} async-done(((bf16[16,576,128]{2,1,0:T(8,128)(2,1)}), bf16[16,576,128]{2,1,0:T(8,128)(2,1)}, u32[]{:S(2)}, u32[]{:S(2)}) %all-to-all-start.2) | async-done | bytes 2359328 | tf_op jit(solution)/shard_map/all_to_all | solution.py:42
  188.0 2.0 reduce_sum.101
  190.0 0.7 reshape.109
  190.7 16.8 %all-to-all-start.3 = ((bf16[32,18,128]{2,1,0:T(8,128)(2,1)}), bf16[32,18,128]{2,1,0:T(8,128)(2,1)}, u32[]{:S(2)}, u32[]{:S(2)}) async-start(bf16[32,18,128]{2,1,0:T(8,128)(2,1)} %reshape.109), calls=%async_computation.3 | async-start | bytes 393216 | tf_op jit(solution)/shard_map/all_to_all | solution.py:167
  208.1 2.7 fusion.7
  210.8 2.5 fusion.2
  213.3 13.1 %all-to-all-done.3 = bf16[32,18,128]{2,1,0:T(8,128)(2,1)} async-done(((bf16[32,18,128]{2,1,0:T(8,128)(2,1)}), bf16[32,18,128]{2,1,0:T(8,128)(2,1)}, u32[]{:S(2)}, u32[]{:S(2)}) %all-to-all-start.3) | async-done | bytes 147488 | tf_op jit(solution)/shard_map/all_to_all | solution.py:167
  226.4 1.0 reshape.110
  227.4 1.0 fusion.6
  229.0 1.2 fusion.4
  230.2 1.0 copy.49
  231.2 4.4 %all-to-all-start.5 = ((bf16[16,64,192]{2,1,0:T(8,128)(2,1)}), bf16[16,64,192]{2,1,0:T(8,128)(2,1)}, u32[]{:S(2)}, u32[]{:S(2)}) async-start(bf16[16,64,192]{2,1,0:T(8,128)(2,1)} %bitcast.139), calls=%async_computation.5 | async-start | bytes 1048576 | tf_op jit(solution)/shard_map/all_to_all | solution.py:42
  235.7 2.7 fusion
  238.4 1.1 convolution_convert_fusion.4
  239.5 6.2 %all-to-all-done.5 = bf16[16,64,192]{2,1,0:T(8,128)(2,1)} async-done(((bf16[16,64,192]{2,1,0:T(8,128)(2,1)}), bf16[16,64,192]{2,1,0:T(8,128)(2,1)}, u32[]{:S(2)}, u32[]{:S(2)}) %all-to-all-start.5) | async-done | bytes 393248 | tf_op jit(solution)/shard_map/all_to_all | solution.py:42
  245.7 5.8 %all-to-all-start.4 = ((bf16[32,32,128]{2,1,0:T(8,128)(2,1)}), bf16[32,32,128]{2,1,0:T(8,128)(2,1)S(1)}, u32[]{:S(2)}, u32[]{:S(2)}) async-start(bf16[32,32,128]{2,1,0:T(8,128)(2,1)} %bitcast.140), calls=%async_computation.4 | async-start | bytes 524288 | tf_op jit(solution)/shard_map/all_to_all | solution.py:42
  251.5 1.1 convert_reduce_fusion
  252.6 2.2 fusion.121
  254.8 7.8 %all-reduce.1 = (f32[192]{0:T(256)}, f32[192]{0:T(256)}) all-reduce(f32[192]{0:T(256)} %get-tuple-element.7, f32[192]{0:T(256)} %get-tuple-element.6), channel_id=1, replica_groups=mesh['sp'=32,'tp_0'=4,'tp_1'=4] {'tp_0'}, use_global_device_ids=true, to_apply=%region_14.15 | all-reduce | flops 384 | bytes 3072 | tf_op jit(solution)/shard_map/psum | solution.py:66
  262.6 7.6 %all-reduce = (f32[192]{0:T(256)}, f32[192]{0:T(256)}) all-reduce(f32[192]{0:T(256)} %get-tuple-element.12, f32[192]{0:T(256)} %get-tuple-element.13), channel_id=1, replica_groups=mesh['sp'=32,'tp_0'=4,'tp_1'=4] {'tp_1'}, use_global_device_ids=true, to_apply=%region_15.16 | all-reduce | flops 384 | bytes 3072 | tf_op jit(solution)/shard_map/psum | solution.py:66
  270.1 0.7 broadcast_multiply_fusion.1
  270.8 0.9 subtract_multiply_fusion
  272.1 5.4 %collective-permute-start = (f32[64,30]{1,0:T(8,128)S(1)}, f32[64,30]{1,0:T(8,128)S(1)}, u32[]{:S(2)}, u32[]{:S(2)}) collective-permute-start(f32[64,30]{1,0:T(8,128)S(1)} %slice.257), channel_id=1, source_target_pairs={{16,0},{32,16},{48,32},{64,48},{80,64},{96,80},{112,96},{128,112},... | collective-permute-start | bytes 23048 | tf_op jit(solution)/shard_map/ppermute | solution.py:73
  277.5 1.7 fusion.1
  279.2 1.2 collective-permute-done
  280.7 1.8 multiply_convert_fusion.6
  (121 shorter events, 6.4 us)
Async XLA Ops:
  7.2 5.5 %copy-start = (bf16[192,2048]{1,0:T(8,128)(2,1)S(1)}, bf16[192,2048]{1,0:T(8,128)(2,1)}, u32[]{:S(2)}) copy-start(bf16[192,2048]{1,0:T(8,128)(2,1)} %param.13) | copy-start | bytes 2359300
  7.2 120.8 %all-gather.2.cloned.1.call-start = ((), (), s32[]{:S(2)}) async-start(), calls=%async_computation.6 | async-start | bytes 6684672 | tf_op jit(solution)/shard_map/all_gather | solution.py:32
  11.5 44.0 %copy-start.12 = (bf16[64,192]{1,0:T(8,128)(2,1)S(1)}, bf16[64,192]{1,0:T(8,128)(2,1)}, u32[]{:S(2)}) copy-start(bf16[64,192]{1,0:T(8,128)(2,1)} %param.24) | copy-start | bytes 73732
  56.4 96.3 %all-to-all-start.1 = ((bf16[16,64,192]{2,1,0:T(8,128)(2,1)}), bf16[16,64,192]{2,1,0:T(8,128)(2,1)}, u32[]{:S(2)}, u32[]{:S(2)}) async-start(bf16[16,64,192]{2,1,0:T(8,128)(2,1)} %broadcast_in_dim.25), calls=%async_computation.1 | async-start | bytes 1048576 | tf_op jit(solution)/shard_map/all_to_all | solution.py:48
  145.9 2.8 copy-start.2
  152.7 4.9 %copy-start.16 = (f32[1024]{0:T(1024)S(1)}, f32[1024]{0:T(1024)}, u32[]{:S(2)}) copy-start(f32[1024]{0:T(1024)} %param.25) | copy-start | bytes 12292
  152.7 5.5 %copy-start.14 = (f32[64,31]{0,1:T(8,128)S(1)}, f32[64,31]{0,1:T(8,128)}, u32[]{:S(2)}) copy-start(f32[64,31]{0,1:T(8,128)} %param.23) | copy-start | bytes 23812
  152.7 35.3 %all-to-all-start.2 = ((bf16[16,576,128]{2,1,0:T(8,128)(2,1)}), bf16[16,576,128]{2,1,0:T(8,128)(2,1)}, u32[]{:S(2)}, u32[]{:S(2)}) async-start(bf16[16,576,128]{2,1,0:T(8,128)(2,1)} %bitcast.138), calls=%async_computation.2 | async-start | bytes 4718592 | tf_op jit(solution)/shard_map/all_to_all | solution.py:42
  190.7 35.7 %all-to-all-start.3 = ((bf16[32,18,128]{2,1,0:T(8,128)(2,1)}), bf16[32,18,128]{2,1,0:T(8,128)(2,1)}, u32[]{:S(2)}, u32[]{:S(2)}) async-start(bf16[32,18,128]{2,1,0:T(8,128)(2,1)} %reshape.109), calls=%async_computation.3 | async-start | bytes 393216 | tf_op jit(solution)/shard_map/all_to_all | solution.py:167
  207.6 3.2 %copy-start.1 = (bf16[576,2048]{1,0:T(8,128)(2,1)S(1)}, bf16[576,2048]{1,0:T(8,128)(2,1)}, u32[]{:S(2)}) copy-start(bf16[576,2048]{1,0:T(8,128)(2,1)} %reshape.107) | copy-start | bytes 7077892
  231.2 14.5 %all-to-all-start.5 = ((bf16[16,64,192]{2,1,0:T(8,128)(2,1)}), bf16[16,64,192]{2,1,0:T(8,128)(2,1)}, u32[]{:S(2)}, u32[]{:S(2)}) async-start(bf16[16,64,192]{2,1,0:T(8,128)(2,1)} %bitcast.139), calls=%async_computation.5 | async-start | bytes 1048576 | tf_op jit(solution)/shard_map/all_to_all | solution.py:42
  235.7 2.7 copy-start.5
  238.4 39.1 %copy-start.7 = (bf16[576,128]{1,0:T(8,128)(2,1)S(1)}, bf16[576,128]{1,0:T(8,128)(2,1)}, u32[]{:S(2)}) copy-start(bf16[576,128]{1,0:T(8,128)(2,1)} %copy-done.6) | copy-start | bytes 442372
  245.7 37.4 %all-to-all-start.4 = ((bf16[32,32,128]{2,1,0:T(8,128)(2,1)}), bf16[32,32,128]{2,1,0:T(8,128)(2,1)S(1)}, u32[]{:S(2)}, u32[]{:S(2)}) async-start(bf16[32,32,128]{2,1,0:T(8,128)(2,1)} %bitcast.140), calls=%async_computation.4 | async-start | bytes 524288 | tf_op jit(solution)/shard_map/all_to_all | solution.py:42
  271.7 8.6 %copy-start.11 = (bf16[64,192]{1,0:T(8,128)(2,1)S(1)}, bf16[64,192]{1,0:T(8,128)(2,1)}, u32[]{:S(2)}) copy-start(bf16[64,192]{1,0:T(8,128)(2,1)} %param.22) | copy-start | bytes 73732
  271.7 8.6 %copy-start.13 = (bf16[64,192]{1,0:T(8,128)(2,1)S(1)}, bf16[64,192]{1,0:T(8,128)(2,1)}, u32[]{:S(2)}) copy-start(bf16[64,192]{1,0:T(8,128)(2,1)} %param.21) | copy-start | bytes 73732
  271.8 8.6 %copy-start.17 = (f32[64]{0:T(128)S(1)}, f32[64]{0:T(128)}, u32[]{:S(2)}) copy-start(f32[64]{0:T(128)} %get-tuple-element.44) | copy-start | bytes 772
  271.8 8.6 %copy-start.18 = (f32[64]{0:T(128)S(1)}, f32[64]{0:T(128)}, u32[]{:S(2)}) copy-start(f32[64]{0:T(128)} %get-tuple-element.45) | copy-start | bytes 772
  271.8 8.6 %copy-start.19 = (f32[64]{0:T(128)S(1)}, f32[64]{0:T(128)}, u32[]{:S(2)}) copy-start(f32[64]{0:T(128)} %get-tuple-element.46) | copy-start | bytes 772
  271.8 8.6 %copy-start.20 = (f32[64]{0:T(128)S(1)}, f32[64]{0:T(128)}, u32[]{:S(2)}) copy-start(f32[64]{0:T(128)} %get-tuple-element.47) | copy-start | bytes 772
  271.8 8.6 %copy-start.21 = (f32[64]{0:T(128)S(1)}, f32[64]{0:T(128)}, u32[]{:S(2)}) copy-start(f32[64]{0:T(128)} %get-tuple-element.48) | copy-start | bytes 772
  271.8 8.6 %copy-start.22 = (f32[64]{0:T(128)S(1)}, f32[64]{0:T(128)}, u32[]{:S(2)}) copy-start(f32[64]{0:T(128)} %get-tuple-element.49) | copy-start | bytes 772
  271.8 8.6 %copy-start.23 = (f32[64]{0:T(128)S(1)}, f32[64]{0:T(128)}, u32[]{:S(2)}) copy-start(f32[64]{0:T(128)} %get-tuple-element.50) | copy-start | bytes 772
  271.8 8.6 %copy-start.24 = (f32[64]{0:T(128)S(1)}, f32[64]{0:T(128)}, u32[]{:S(2)}) copy-start(f32[64]{0:T(128)} %get-tuple-element.51) | copy-start | bytes 772
  271.8 8.6 %copy-start.25 = (f32[64]{0:T(128)S(1)}, f32[64]{0:T(128)}, u32[]{:S(2)}) copy-start(f32[64]{0:T(128)} %get-tuple-element.52) | copy-start | bytes 772
  271.8 8.6 %copy-start.26 = (f32[64]{0:T(128)S(1)}, f32[64]{0:T(128)}, u32[]{:S(2)}) copy-start(f32[64]{0:T(128)} %get-tuple-element.53) | copy-start | bytes 772
  271.9 8.6 %copy-start.27 = (f32[64]{0:T(128)S(1)}, f32[64]{0:T(128)}, u32[]{:S(2)}) copy-start(f32[64]{0:T(128)} %get-tuple-element.54) | copy-start | bytes 772
  271.9 8.6 %copy-start.28 = (f32[64]{0:T(128)S(1)}, f32[64]{0:T(128)}, u32[]{:S(2)}) copy-start(f32[64]{0:T(128)} %get-tuple-element.55) | copy-start | bytes 772
  271.9 8.6 %copy-start.29 = (f32[64]{0:T(128)S(1)}, f32[64]{0:T(128)}, u32[]{:S(2)}) copy-start(f32[64]{0:T(128)} %get-tuple-element.25) | copy-start | bytes 772
  271.9 8.6 %copy-start.30 = (f32[64]{0:T(128)S(1)}, f32[64]{0:T(128)}, u32[]{:S(2)}) copy-start(f32[64]{0:T(128)} %get-tuple-element.26) | copy-start | bytes 772
  271.9 8.6 %copy-start.31 = (f32[64]{0:T(128)S(1)}, f32[64]{0:T(128)}, u32[]{:S(2)}) copy-start(f32[64]{0:T(128)} %get-tuple-element.27) | copy-start | bytes 772
  271.9 8.6 %copy-start.32 = (f32[64]{0:T(128)S(1)}, f32[64]{0:T(128)}, u32[]{:S(2)}) copy-start(f32[64]{0:T(128)} %get-tuple-element.28) | copy-start | bytes 772
  271.9 8.6 %copy-start.33 = (f32[64]{0:T(128)S(1)}, f32[64]{0:T(128)}, u32[]{:S(2)}) copy-start(f32[64]{0:T(128)} %get-tuple-element.29) | copy-start | bytes 772
  271.9 8.6 %copy-start.34 = (f32[64]{0:T(128)S(1)}, f32[64]{0:T(128)}, u32[]{:S(2)}) copy-start(f32[64]{0:T(128)} %get-tuple-element.30) | copy-start | bytes 772
  271.9 8.6 %copy-start.35 = (f32[64]{0:T(128)S(1)}, f32[64]{0:T(128)}, u32[]{:S(2)}) copy-start(f32[64]{0:T(128)} %get-tuple-element.31) | copy-start | bytes 772
  271.9 8.6 %copy-start.36 = (f32[64]{0:T(128)S(1)}, f32[64]{0:T(128)}, u32[]{:S(2)}) copy-start(f32[64]{0:T(128)} %get-tuple-element.32) | copy-start | bytes 772
  272.0 8.6 %copy-start.37 = (f32[64]{0:T(128)S(1)}, f32[64]{0:T(128)}, u32[]{:S(2)}) copy-start(f32[64]{0:T(128)} %get-tuple-element.33) | copy-start | bytes 772
  272.0 8.6 %copy-start.38 = (f32[64]{0:T(128)S(1)}, f32[64]{0:T(128)}, u32[]{:S(2)}) copy-start(f32[64]{0:T(128)} %get-tuple-element.34) | copy-start | bytes 772
  272.0 8.6 %copy-start.39 = (f32[64]{0:T(128)S(1)}, f32[64]{0:T(128)}, u32[]{:S(2)}) copy-start(f32[64]{0:T(128)} %get-tuple-element.35) | copy-start | bytes 772
  272.0 8.6 %copy-start.40 = (f32[64]{0:T(128)S(1)}, f32[64]{0:T(128)}, u32[]{:S(2)}) copy-start(f32[64]{0:T(128)} %get-tuple-element.36) | copy-start | bytes 772
  272.0 8.6 %copy-start.41 = (f32[64]{0:T(128)S(1)}, f32[64]{0:T(128)}, u32[]{:S(2)}) copy-start(f32[64]{0:T(128)} %get-tuple-element.37) | copy-start | bytes 772
  272.0 8.6 %copy-start.42 = (f32[64]{0:T(128)S(1)}, f32[64]{0:T(128)}, u32[]{:S(2)}) copy-start(f32[64]{0:T(128)} %get-tuple-element.38) | copy-start | bytes 772
  272.0 8.6 %copy-start.43 = (f32[64]{0:T(128)S(1)}, f32[64]{0:T(128)}, u32[]{:S(2)}) copy-start(f32[64]{0:T(128)} %get-tuple-element.39) | copy-start | bytes 772
  272.0 8.6 %copy-start.44 = (f32[64]{0:T(128)S(1)}, f32[64]{0:T(128)}, u32[]{:S(2)}) copy-start(f32[64]{0:T(128)} %get-tuple-element.40) | copy-start | bytes 772
  272.0 8.6 %copy-start.45 = (f32[64]{0:T(128)S(1)}, f32[64]{0:T(128)}, u32[]{:S(2)}) copy-start(f32[64]{0:T(128)} %get-tuple-element.41) | copy-start | bytes 772
  272.0 8.6 %copy-start.46 = (f32[64]{0:T(128)S(1)}, f32[64]{0:T(128)}, u32[]{:S(2)}) copy-start(f32[64]{0:T(128)} %get-tuple-element.42) | copy-start | bytes 772
  272.1 8.6 %copy-start.47 = (f32[64]{0:T(128)S(1)}, f32[64]{0:T(128)}, u32[]{:S(2)}) copy-start(f32[64]{0:T(128)} %get-tuple-element.43) | copy-start | bytes 772
  272.1 8.3 %collective-permute-start = (f32[64,30]{1,0:T(8,128)S(1)}, f32[64,30]{1,0:T(8,128)S(1)}, u32[]{:S(2)}, u32[]{:S(2)}) collective-permute-start(f32[64,30]{1,0:T(8,128)S(1)} %slice.257), channel_id=1, source_target_pairs={{16,0},{32,16},{48,32},{64,48},{80,64},{96,80},{112,96},{128,112},... | collective-permute-start | bytes 23048 | tf_op jit(solution)/shard_map/ppermute | solution.py:73
  (7 other events, 9.3 us)
Sparse Core Ops, SparseCore 0:
  55.7 72.2 all-gather.1
where the time goes:
time: 292 us; the launch traced here: 291 us
  waiting for transfers between devices  111 us (38%)
  blocking collectives  56.9 us (19%)
  starting transfers between devices  44.1 us (15%)
  local copies, waits for them, and re-layouts  24.8 us (8%)
  matrix products  20 us (7%)
  other arithmetic  18.6 us (6%)
  between operations  14.9 us (5%)
    all_gather x1, waiting for transfers between devices, sent_together_2(): lax.all_gather(both, axis, axis=dim, tiled=True)  64.7 us
    all_to_all x1, blocking collectives, sent_together(): lax.all_to_all(both, axis, split_axis=split_dim, concat_axis=concat_dim,...  41.5 us
    all_to_all x3, waiting for transfers between devices, sum_at_owner(): lax.all_to_all(in_blocks(shard, dim, length), axis, 0, 0, tiled=True)  32.2 us
    all_to_all x1, starting transfers between devices, body(): lax.all_to_all(summed_grad.reshape(groups, capacity, part_width), 'sp', s...  16.8 us
    psum x2, blocking collectives, over_axes(): shard = lax.psum(shard, axis)  15.4 us
    all_to_all x3, starting transfers between devices, sum_at_owner(): lax.all_to_all(in_blocks(shard, dim, length), axis, 0, 0, tiled=True)  15 us
    all_to_all x1, waiting for transfers between devices, body(): lax.all_to_all(summed_grad.reshape(groups, capacity, part_width), 'sp', s...  13.1 us
    all_to_all x1, starting transfers between devices, from_everyone(): lax.all_to_all(jnp.broadcast_to(shard[None], (length, *shard.shape)), axi...  6.81 us
  transfers between devices with their start and end apart: 7, of which 5 were waited for; matrix products, arithmetic and copies ran while one was open for 16% of the time, Pallas kernels for 0%

commit v1 on v0

--- a/solution.py
+++ b/solution.py
@@ -63,7 +63,7 @@
 
 def over_axes(shard, axes):
     for axis in axes:
-        shard = lax.psum(shard, axis)
+        shard = jnp.sum(lax.all_gather(shard, axis), axis=0)
     return shard
 
 

time: 292 us -> 311 us (1.065)
  local copies, waits for them, and re-layouts: 24.8 us -> 40.6 us
  other arithmetic: 18.6 us -> 23.7 us
  waiting for transfers between devices: 111 us -> 107 us
    psum x2 -> x0, blocking collectives: 15.4 us -> none  [over_axes(): shard = lax.psum(shard, axis)]
    unnamed x0 -> x2, blocking collectives: none -> 15.3 us
    unnamed x97 -> x107, local copies, waits for them, and re-layouts: 2.54 us -> 13 us
    all_gather x0 -> x4, local copies, waits for them, and re-layouts: none -> 5.42 us  [over_axes(): shard = jnp.sum(lax.all_gather(shard, axis), axis=0)]
    reduce_sum x0 -> x4, other arithmetic: none -> 5.06 us  [over_axes(): shard = jnp.sum(lax.all_gather(shard, axis), axis=0)]
    all_to_all x3, waiting for transfers between devices: 32.2 us -> 28.4 us  [sum_at_owner(): lax.all_to_all(in_blocks(shard, dim, length), axis, 0, 0, tiled=True)]
  transfers between devices with their start and end apart: 7 -> 7, of which waited for: 5 -> 5; matrix products, arithmetic and copies ran while one was open for 16% -> 22% of each run, Pallas kernels for 0% -> 0%
where the time goes in v1:
time: 311 us; the launch traced here: 309 us
  waiting for transfers between devices  107 us (34%)
  blocking collectives  56.8 us (18%)
  starting transfers between devices  44.4 us (14%)
  local copies, waits for them, and re-layouts  40.6 us (13%)
  other arithmetic  23.7 us (8%)
  matrix products  20 us (6%)
  between operations  16.2 us (5%)
    all_gather x1, waiting for transfers between devices, sent_together_2(): lax.all_gather(both, axis, axis=dim, tiled=True)  64.7 us
    all_to_all x1, blocking collectives, sent_together(): lax.all_to_all(both, axis, split_axis=split_dim, concat_axis=concat_dim,...  41.5 us
    all_to_all x3, waiting for transfers between devices, sum_at_owner(): lax.all_to_all(in_blocks(shard, dim, length), axis, 0, 0, tiled=True)  28.4 us
    all_to_all x1, starting transfers between devices, body(): lax.all_to_all(summed_grad.reshape(groups, capacity, part_width), 'sp', s...  16.8 us
    unnamed x2, blocking collectives  15.3 us
    all_to_all x3, starting transfers between devices, sum_at_owner(): lax.all_to_all(in_blocks(shard, dim, length), axis, 0, 0, tiled=True)  15 us
    all_to_all x1, waiting for transfers between devices, body(): lax.all_to_all(summed_grad.reshape(groups, capacity, part_width), 'sp', s...  13.1 us
    unnamed x107, local copies, waits for them, and re-layouts  13 us
  transfers between devices with their start and end apart: 7, of which 5 were waited for; matrix products, arithmetic and copies ran while one was open for 22% of the time, Pallas kernels for 0%

profile of v1, /device:TPU:1, one launch (start us, length us, event | category | flops | bytes accessed | tf_op | source)
XLA Modules:
  0.0 309.2 jit_solution(10044723152118392922)
XLA Ops:
  11.5 1.1 fusion.5
  13.1 41.5 %all_to_all.30 = bf16[32,36,128]{2,1,0:T(8,128)(2,1)S(1)} all-to-all(bf16[32,36,128]{2,1,0:T(8,128)(2,1)S(1)} %pad_maximum_fusion.1), channel_id=1, replica_groups=mesh['sp'=32,'tp_0'=4,'tp_1'=4] {'sp'}, dimensions={0} | all-to-all | bytes 589824 | tf_op jit(solution)/shard_map/all_to_all | solution.py:19
  56.4 6.8 %all-to-all-start.1 = ((bf16[16,64,192]{2,1,0:T(8,128)(2,1)}), bf16[16,64,192]{2,1,0:T(8,128)(2,1)}, u32[]{:S(2)}, u32[]{:S(2)}) async-start(bf16[16,64,192]{2,1,0:T(8,128)(2,1)} %broadcast_in_dim.25), calls=%async_computation.1 | async-start | bytes 1048576 | tf_op jit(solution)/shard_map/all_to_all | solution.py:48
  63.2 64.7 %all-gather.6.cloned.1.call-done = bf16[64,18,2048]{2,1,0:T(8,128)(2,1)} async-done(((bf16[64,18,128]{2,1,0:T(8,128)(2,1)}), bf16[64,18,2048]{2,1,0:T(8,128)(2,1)}) %all-gather.6.cloned.1.call-update) | async-done | bytes 4718608 | tf_op jit(solution)/shard_map/all_gather | solution.py:32
  128.0 6.6 %fusion.123 = (bf16[32,18,2048]{2,1,0:T(8,128)(2,1)}, bf16[32,18,2048]{2,1,0:T(8,128)(2,1)}) fusion(bf16[64,18,2048]{2,1,0:T(8,128)(2,1)} %all-gather.6.cloned.1.call-done), kind=kLoop, calls=%fused_computation.232 | loop fusion | bytes 9437184 | tf_op jit(solution)/shard_map/split | solution.py:32
  134.6 2.9 reshape.110
  137.5 2.6 fusion.10
  140.1 1.5 fusion.13
  141.6 4.3 %reshape.111 = bf16[576,2048]{1,0:T(8,128)(2,1)} reshape(bf16[32,18,2048]{2,1,0:T(8,128)(2,1)} %get-tuple-element.17) | data formatting | bytes 4718592 | tf_op jit(solution)/shard_map/reshape | solution.py:138
  145.9 2.8 multiply_convert_fusion.3
  150.7 2.1 copy.54
  152.7 4.8 %all-to-all-start.2 = ((bf16[16,576,128]{2,1,0:T(8,128)(2,1)}), bf16[16,576,128]{2,1,0:T(8,128)(2,1)}, u32[]{:S(2)}, u32[]{:S(2)}) async-start(bf16[16,576,128]{2,1,0:T(8,128)(2,1)} %bitcast.140), calls=%async_computation.2 | async-start | bytes 4718592 | tf_op jit(solution)/shard_map/all_to_all | solution.py:42
  157.6 1.3 dynamic-slice
  158.9 1.3 dynamic-slice.1
  163.3 1.2 convert_reduce_fusion.2
  164.5 1.2 multiply_reduce_fusion
  165.8 22.2 %all-to-all-done.2 = bf16[16,576,128]{2,1,0:T(8,128)(2,1)} async-done(((bf16[16,576,128]{2,1,0:T(8,128)(2,1)}), bf16[16,576,128]{2,1,0:T(8,128)(2,1)}, u32[]{:S(2)}, u32[]{:S(2)}) %all-to-all-start.2) | async-done | bytes 2359328 | tf_op jit(solution)/shard_map/all_to_all | solution.py:42
  188.0 2.0 reduce_sum.137
  190.7 16.8 %all-to-all-start.3 = ((bf16[32,18,128]{2,1,0:T(8,128)(2,1)}), bf16[32,18,128]{2,1,0:T(8,128)(2,1)}, u32[]{:S(2)}, u32[]{:S(2)}) async-start(bf16[32,18,128]{2,1,0:T(8,128)(2,1)} %reshape.113), calls=%async_computation.3 | async-start | bytes 393216 | tf_op jit(solution)/shard_map/all_to_all | solution.py:167
  208.2 2.6 fusion.7
  210.8 2.5 fusion.2
  213.3 13.1 %all-to-all-done.3 = bf16[32,18,128]{2,1,0:T(8,128)(2,1)} async-done(((bf16[32,18,128]{2,1,0:T(8,128)(2,1)}), bf16[32,18,128]{2,1,0:T(8,128)(2,1)}, u32[]{:S(2)}, u32[]{:S(2)}) %all-to-all-start.3) | async-done | bytes 147488 | tf_op jit(solution)/shard_map/all_to_all | solution.py:167
  229.0 1.2 fusion.4
  231.2 4.4 %all-to-all-start.5 = ((bf16[16,64,192]{2,1,0:T(8,128)(2,1)}), bf16[16,64,192]{2,1,0:T(8,128)(2,1)}, u32[]{:S(2)}, u32[]{:S(2)}) async-start(bf16[16,64,192]{2,1,0:T(8,128)(2,1)} %bitcast.141), calls=%async_computation.5 | async-start | bytes 1048576 | tf_op jit(solution)/shard_map/all_to_all | solution.py:42
  235.7 2.7 fusion
  238.4 1.1 convolution_convert_fusion.4
  239.5 6.2 %all-to-all-done.5 = bf16[16,64,192]{2,1,0:T(8,128)(2,1)} async-done(((bf16[16,64,192]{2,1,0:T(8,128)(2,1)}), bf16[16,64,192]{2,1,0:T(8,128)(2,1)}, u32[]{:S(2)}, u32[]{:S(2)}) %all-to-all-start.5) | async-done | bytes 393248 | tf_op jit(solution)/shard_map/all_to_all | solution.py:42
  245.7 5.8 %all-to-all-start.4 = ((bf16[32,32,128]{2,1,0:T(8,128)(2,1)}), bf16[32,32,128]{2,1,0:T(8,128)(2,1)S(1)}, u32[]{:S(2)}, u32[]{:S(2)}) async-start(bf16[32,32,128]{2,1,0:T(8,128)(2,1)} %bitcast.142), calls=%async_computation.4 | async-start | bytes 524288 | tf_op jit(solution)/shard_map/all_to_all | solution.py:42
  251.5 1.1 convert_reduce_fusion
  252.6 2.2 fusion.121
  255.4 1.4 dynamic-update-slice.2
  257.4 1.4 dynamic-update-slice
  258.7 7.9 %all-reduce.5 = (f32[768]{0:T(1024)}, f32[768]{0:T(1024)}) all-reduce(f32[768]{0:T(1024)} %dynamic-update-slice.2, f32[768]{0:T(1024)} %dynamic-update-slice), channel_id=4, replica_groups=mesh['sp'=32,'tp_0'=4,'tp_1'=4] {'tp_0'}, use_global_device_ids=true, to_apply=%add.2 | all-reduce | flops 1536 | bytes 12288
  266.7 1.4 reshape.120
  268.0 1.4 reshape.118
  269.4 1.3 reduce_sum.144
  270.6 1.3 reduce_sum.141
  272.5 1.4 dynamic-update-slice.3
  274.5 1.4 dynamic-update-slice.1
  275.8 7.4 %all-reduce.4 = (f32[768]{0:T(1024)}, f32[768]{0:T(1024)}) all-reduce(f32[768]{0:T(1024)} %dynamic-update-slice.3, f32[768]{0:T(1024)} %dynamic-update-slice.1), channel_id=5, replica_groups=mesh['sp'=32,'tp_0'=4,'tp_1'=4] {'tp_1'}, use_global_device_ids=true, to_apply=%add.3 | all-reduce | flops 1536 | bytes 12288
  283.2 1.4 reshape.121
  284.6 1.4 reshape.119
  285.9 1.3 reduce_sum.145
  287.2 1.3 reduce_sum.142
  290.4 5.7 %collective-permute-start = (f32[64,30]{1,0:T(8,128)S(1)}, f32[64,30]{1,0:T(8,128)S(1)}, u32[]{:S(2)}, u32[]{:S(2)}) collective-permute-start(f32[64,30]{1,0:T(8,128)S(1)} %slice.257), channel_id=1, source_target_pairs={{16,0},{32,16},{48,32},{64,48},{80,64},{96,80},{112,96},{128,112},... | collective-permute-start | bytes 23048 | tf_op jit(solution)/shard_map/ppermute | solution.py:73
  296.1 1.7 fusion.1
  297.8 1.2 collective-permute-done
  299.3 1.8 multiply_convert_fusion.6
  (139 shorter events, 20.6 us)
Async XLA Ops:
  7.2 5.5 %copy-start = (bf16[192,2048]{1,0:T(8,128)(2,1)S(1)}, bf16[192,2048]{1,0:T(8,128)(2,1)}, u32[]{:S(2)}) copy-start(bf16[192,2048]{1,0:T(8,128)(2,1)} %param.13) | copy-start | bytes 2359300
  7.2 120.8 %all-gather.6.cloned.1.call-start = ((), (), s32[]{:S(2)}) async-start(), calls=%async_computation.6 | async-start | bytes 6684672 | tf_op jit(solution)/shard_map/all_gather | solution.py:32
  11.5 44.0 %copy-start.12 = (bf16[64,192]{1,0:T(8,128)(2,1)S(1)}, bf16[64,192]{1,0:T(8,128)(2,1)}, u32[]{:S(2)}) copy-start(bf16[64,192]{1,0:T(8,128)(2,1)} %param.24) | copy-start | bytes 73732
  56.4 96.3 %all-to-all-start.1 = ((bf16[16,64,192]{2,1,0:T(8,128)(2,1)}), bf16[16,64,192]{2,1,0:T(8,128)(2,1)}, u32[]{:S(2)}, u32[]{:S(2)}) async-start(bf16[16,64,192]{2,1,0:T(8,128)(2,1)} %broadcast_in_dim.25), calls=%async_computation.1 | async-start | bytes 1048576 | tf_op jit(solution)/shard_map/all_to_all | solution.py:48
  145.9 2.8 copy-start.2
  152.7 8.7 %copy-start.16 = (f32[1024]{0:T(1024)S(1)}, f32[1024]{0:T(1024)}, u32[]{:S(2)}) copy-start(f32[1024]{0:T(1024)} %param.25) | copy-start | bytes 12292
  152.7 9.3 %copy-start.14 = (f32[64,31]{0,1:T(8,128)S(1)}, f32[64,31]{0,1:T(8,128)}, u32[]{:S(2)}) copy-start(f32[64,31]{0,1:T(8,128)} %param.23) | copy-start | bytes 23812
  152.7 35.3 %all-to-all-start.2 = ((bf16[16,576,128]{2,1,0:T(8,128)(2,1)}), bf16[16,576,128]{2,1,0:T(8,128)(2,1)}, u32[]{:S(2)}, u32[]{:S(2)}) async-start(bf16[16,576,128]{2,1,0:T(8,128)(2,1)} %bitcast.140), calls=%async_computation.2 | async-start | bytes 4718592 | tf_op jit(solution)/shard_map/all_to_all | solution.py:42
  190.7 35.7 %all-to-all-start.3 = ((bf16[32,18,128]{2,1,0:T(8,128)(2,1)}), bf16[32,18,128]{2,1,0:T(8,128)(2,1)}, u32[]{:S(2)}, u32[]{:S(2)}) async-start(bf16[32,18,128]{2,1,0:T(8,128)(2,1)} %reshape.113), calls=%async_computation.3 | async-start | bytes 393216 | tf_op jit(solution)/shard_map/all_to_all | solution.py:167
  207.6 3.2 %copy-start.1 = (bf16[576,2048]{1,0:T(8,128)(2,1)S(1)}, bf16[576,2048]{1,0:T(8,128)(2,1)}, u32[]{:S(2)}) copy-start(bf16[576,2048]{1,0:T(8,128)(2,1)} %reshape.111) | copy-start | bytes 7077892
  231.2 14.5 %all-to-all-start.5 = ((bf16[16,64,192]{2,1,0:T(8,128)(2,1)}), bf16[16,64,192]{2,1,0:T(8,128)(2,1)}, u32[]{:S(2)}, u32[]{:S(2)}) async-start(bf16[16,64,192]{2,1,0:T(8,128)(2,1)} %bitcast.141), calls=%async_computation.5 | async-start | bytes 1048576 | tf_op jit(solution)/shard_map/all_to_all | solution.py:42
  235.7 2.7 copy-start.5
  238.4 57.7 %copy-start.7 = (bf16[576,128]{1,0:T(8,128)(2,1)S(1)}, bf16[576,128]{1,0:T(8,128)(2,1)}, u32[]{:S(2)}) copy-start(bf16[576,128]{1,0:T(8,128)(2,1)} %copy-done.6) | copy-start | bytes 442372
  245.7 56.0 %all-to-all-start.4 = ((bf16[32,32,128]{2,1,0:T(8,128)(2,1)}), bf16[32,32,128]{2,1,0:T(8,128)(2,1)S(1)}, u32[]{:S(2)}, u32[]{:S(2)}) async-start(bf16[32,32,128]{2,1,0:T(8,128)(2,1)} %bitcast.142), calls=%async_computation.4 | async-start | bytes 524288 | tf_op jit(solution)/shard_map/all_to_all | solution.py:42
  290.1 8.9 %copy-start.11 = (bf16[64,192]{1,0:T(8,128)(2,1)S(1)}, bf16[64,192]{1,0:T(8,128)(2,1)}, u32[]{:S(2)}) copy-start(bf16[64,192]{1,0:T(8,128)(2,1)} %param.22) | copy-start | bytes 73732
  290.1 8.9 %copy-start.13 = (bf16[64,192]{1,0:T(8,128)(2,1)S(1)}, bf16[64,192]{1,0:T(8,128)(2,1)}, u32[]{:S(2)}) copy-start(bf16[64,192]{1,0:T(8,128)(2,1)} %param.21) | copy-start | bytes 73732
  290.1 8.9 %copy-start.17 = (f32[64]{0:T(128)S(1)}, f32[64]{0:T(128)}, u32[]{:S(2)}) copy-start(f32[64]{0:T(128)} %get-tuple-element.44) | copy-start | bytes 772
  290.1 8.9 %copy-start.18 = (f32[64]{0:T(128)S(1)}, f32[64]{0:T(128)}, u32[]{:S(2)}) copy-start(f32[64]{0:T(128)} %get-tuple-element.45) | copy-start | bytes 772
  290.1 8.9 %copy-start.19 = (f32[64]{0:T(128)S(1)}, f32[64]{0:T(128)}, u32[]{:S(2)}) copy-start(f32[64]{0:T(128)} %get-tuple-element.46) | copy-start | bytes 772
  290.1 8.9 %copy-start.20 = (f32[64]{0:T(128)S(1)}, f32[64]{0:T(128)}, u32[]{:S(2)}) copy-start(f32[64]{0:T(128)} %get-tuple-element.47) | copy-start | bytes 772
  290.1 8.9 %copy-start.21 = (f32[64]{0:T(128)S(1)}, f32[64]{0:T(128)}, u32[]{:S(2)}) copy-start(f32[64]{0:T(128)} %get-tuple-element.48) | copy-start | bytes 772
  290.1 8.9 %copy-start.22 = (f32[64]{0:T(128)S(1)}, f32[64]{0:T(128)}, u32[]{:S(2)}) copy-start(f32[64]{0:T(128)} %get-tuple-element.49) | copy-start | bytes 772
  290.1 8.9 %copy-start.23 = (f32[64]{0:T(128)S(1)}, f32[64]{0:T(128)}, u32[]{:S(2)}) copy-start(f32[64]{0:T(128)} %get-tuple-element.50) | copy-start | bytes 772
  290.2 8.9 %copy-start.24 = (f32[64]{0:T(128)S(1)}, f32[64]{0:T(128)}, u32[]{:S(2)}) copy-start(f32[64]{0:T(128)} %get-tuple-element.51) | copy-start | bytes 772
  290.2 8.9 %copy-start.25 = (f32[64]{0:T(128)S(1)}, f32[64]{0:T(128)}, u32[]{:S(2)}) copy-start(f32[64]{0:T(128)} %get-tuple-element.52) | copy-start | bytes 772
  290.2 8.9 %copy-start.26 = (f32[64]{0:T(128)S(1)}, f32[64]{0:T(128)}, u32[]{:S(2)}) copy-start(f32[64]{0:T(128)} %get-tuple-element.53) | copy-start | bytes 772
  290.2 8.9 %copy-start.27 = (f32[64]{0:T(128)S(1)}, f32[64]{0:T(128)}, u32[]{:S(2)}) copy-start(f32[64]{0:T(128)} %get-tuple-element.54) | copy-start | bytes 772
  290.2 8.9 %copy-start.28 = (f32[64]{0:T(128)S(1)}, f32[64]{0:T(128)}, u32[]{:S(2)}) copy-start(f32[64]{0:T(128)} %get-tuple-element.55) | copy-start | bytes 772
  290.2 8.9 %copy-start.29 = (f32[64]{0:T(128)S(1)}, f32[64]{0:T(128)}, u32[]{:S(2)}) copy-start(f32[64]{0:T(128)} %get-tuple-element.25) | copy-start | bytes 772
  290.2 8.9 %copy-start.30 = (f32[64]{0:T(128)S(1)}, f32[64]{0:T(128)}, u32[]{:S(2)}) copy-start(f32[64]{0:T(128)} %get-tuple-element.26) | copy-start | bytes 772
  290.2 8.9 %copy-start.31 = (f32[64]{0:T(128)S(1)}, f32[64]{0:T(128)}, u32[]{:S(2)}) copy-start(f32[64]{0:T(128)} %get-tuple-element.27) | copy-start | bytes 772
  290.2 8.9 %copy-start.32 = (f32[64]{0:T(128)S(1)}, f32[64]{0:T(128)}, u32[]{:S(2)}) copy-start(f32[64]{0:T(128)} %get-tuple-element.28) | copy-start | bytes 772
  290.2 8.9 %copy-start.33 = (f32[64]{0:T(128)S(1)}, f32[64]{0:T(128)}, u32[]{:S(2)}) copy-start(f32[64]{0:T(128)} %get-tuple-element.29) | copy-start | bytes 772
  290.3 8.9 %copy-start.34 = (f32[64]{0:T(128)S(1)}, f32[64]{0:T(128)}, u32[]{:S(2)}) copy-start(f32[64]{0:T(128)} %get-tuple-element.30) | copy-start | bytes 772
  290.3 8.9 %copy-start.35 = (f32[64]{0:T(128)S(1)}, f32[64]{0:T(128)}, u32[]{:S(2)}) copy-start(f32[64]{0:T(128)} %get-tuple-element.31) | copy-start | bytes 772
  290.3 8.9 %copy-start.36 = (f32[64]{0:T(128)S(1)}, f32[64]{0:T(128)}, u32[]{:S(2)}) copy-start(f32[64]{0:T(128)} %get-tuple-element.32) | copy-start | bytes 772
  290.3 8.9 %copy-start.37 = (f32[64]{0:T(128)S(1)}, f32[64]{0:T(128)}, u32[]{:S(2)}) copy-start(f32[64]{0:T(128)} %get-tuple-element.33) | copy-start | bytes 772
  290.3 8.9 %copy-start.38 = (f32[64]{0:T(128)S(1)}, f32[64]{0:T(128)}, u32[]{:S(2)}) copy-start(f32[64]{0:T(128)} %get-tuple-element.34) | copy-start | bytes 772
  290.3 8.9 %copy-start.39 = (f32[64]{0:T(128)S(1)}, f32[64]{0:T(128)}, u32[]{:S(2)}) copy-start(f32[64]{0:T(128)} %get-tuple-element.35) | copy-start | bytes 772
  290.3 8.9 %copy-start.40 = (f32[64]{0:T(128)S(1)}, f32[64]{0:T(128)}, u32[]{:S(2)}) copy-start(f32[64]{0:T(128)} %get-tuple-element.36) | copy-start | bytes 772
  290.3 8.9 %copy-start.41 = (f32[64]{0:T(128)S(1)}, f32[64]{0:T(128)}, u32[]{:S(2)}) copy-start(f32[64]{0:T(128)} %get-tuple-element.37) | copy-start | bytes 772
  290.3 8.9 %copy-start.42 = (f32[64]{0:T(128)S(1)}, f32[64]{0:T(128)}, u32[]{:S(2)}) copy-start(f32[64]{0:T(128)} %get-tuple-element.38) | copy-start | bytes 772
  290.3 8.9 %copy-start.43 = (f32[64]{0:T(128)S(1)}, f32[64]{0:T(128)}, u32[]{:S(2)}) copy-start(f32[64]{0:T(128)} %get-tuple-element.39) | copy-start | bytes 772
  290.4 8.9 %copy-start.44 = (f32[64]{0:T(128)S(1)}, f32[64]{0:T(128)}, u32[]{:S(2)}) copy-start(f32[64]{0:T(128)} %get-tuple-element.40) | copy-start | bytes 772
  290.4 8.9 %copy-start.45 = (f32[64]{0:T(128)S(1)}, f32[64]{0:T(128)}, u32[]{:S(2)}) copy-start(f32[64]{0:T(128)} %get-tuple-element.41) | copy-start | bytes 772
  290.4 8.9 %copy-start.46 = (f32[64]{0:T(128)S(1)}, f32[64]{0:T(128)}, u32[]{:S(2)}) copy-start(f32[64]{0:T(128)} %get-tuple-element.42) | copy-start | bytes 772
  290.4 8.9 %copy-start.47 = (f32[64]{0:T(128)S(1)}, f32[64]{0:T(128)}, u32[]{:S(2)}) copy-start(f32[64]{0:T(128)} %get-tuple-element.43) | copy-start | bytes 772
  290.4 8.6 %collective-permute-start = (f32[64,30]{1,0:T(8,128)S(1)}, f32[64,30]{1,0:T(8,128)S(1)}, u32[]{:S(2)}, u32[]{:S(2)}) collective-permute-start(f32[64,30]{1,0:T(8,128)S(1)} %slice.257), channel_id=1, source_target_pairs={{16,0},{32,16},{48,32},{64,48},{80,64},{96,80},{112,96},{128,112},... | collective-permute-start | bytes 23048 | tf_op jit(solution)/shard_map/ppermute | solution.py:73
  (7 other events, 9.3 us)
Sparse Core Ops, SparseCore 0:
  55.7 72.2 all-gather.5
